TPU v7x, 32 devices: a whole 2x2x4 slice. The times are simulated.
32 devices in a mesh: ep: 4 (over y, x), tp: 8 (over z, core).
Axes of the slice: x: 2, y: 2, z: 4, core: 2. Of those that a mesh axis runs over, the one named last changes fastest.
Arguments:
- tokens: bfloat16 [64, 4096], P('ep'), may hold values from -6 to 6
- attn_gain: float32 [4096], replicated, may hold values from 0.1 to 1.9
- w_query: bfloat16 [4096, 2048], P('ep', 'tp'), may hold values from -0.15625 to 0.15625
- w_key: bfloat16 [4096, 2048], P('ep', 'tp'), may hold values from -0.09375 to 0.09375
- w_value: bfloat16 [4096, 2048], P('ep', 'tp'), may hold values from -0.09375 to 0.09375
- mix_lambda: float32 [16], P('tp'), may hold values from 0.3 to 0.8
- head_gain: float32 [128], replicated, may hold values from 0.1 to 1.9
- w_output: bfloat16 [2048, 4096], P('tp'), may hold values from -0.125 to 0.125
- cache_keys: bfloat16 [64, 1024, 2048], P('ep', None, 'tp'), may hold values from -180 to 180
- cache_value: bfloat16 [64, 1024, 2048], P('ep', None, 'tp'), may hold values from -6 to 6
- lengths: int32 [64], P('ep'), may hold values from 1 to 1024
- moe_gain: float32 [4096], replicated, may hold values from 0.1 to 1.9
- group_ids: int32 [64], P('ep'), may hold values from 0 to 1, as said below
- member_ids: int32 [64, 2], P('ep'), may hold values from 0 to 1, as said below
- group_gate: float32 [64], P('ep'), may hold values from 0.3 to 1
- member_logits: float32 [64, 2], P('ep'), may hold values from -4 to 4
- w_exp_gate: bfloat16 [4, 4096, 2048], P('ep', None, 'tp'), may hold values from -0.09375 to 0.09375
- w_exp_up: bfloat16 [4, 4096, 2048], P('ep', None, 'tp'), may hold values from -0.09375 to 0.09375
- w_exp_down: bfloat16 [4, 2048, 4096], P('ep', 'tp'), may hold values from -0.125 to 0.125
Outputs:
- mixed: bfloat16 [64, 4096], P('ep', 'tp')
- fresh_keys: bfloat16 [64, 2048], P('ep', 'tp')
- fresh_value: bfloat16 [64, 2048], P('ep', 'tp')
Inputs may be any that keep to these rules, and one draw needn't show every extreme that they name: `group_ids`: each index of ep holds 16 consecutive tokens, of which every group gets the same number. A token's 2 members differ, and every expert group_ids * 2 + member_ids receives exactly 8 of the token-expert pairs of each index of ep.
All inputs are finite; a program needn't handle non-finite values.
Results may differ from a plain program's by a relative error of at most 0.015.
The roundings to bfloat16 on the way count: a program that leaves them out, or rounds other values in their place, can miss the bound.
Values may be sent and summed in bfloat16 or wider, within the bound.
No kernel may reach another device: no remote copies, remote signals or barrier semaphores. Data moves between devices by JAX's collectives and lax.ppermute only.
A program may use at most 64 MiB of HBM per device.

v0:
```python
import jax
import jax.numpy as jnp
from jax import lax
from jax.sharding import PartitionSpec as P

EPG = 2


EPS = 1e-06


def rms_scale(values, gain):
    return values * lax.rsqrt(jnp.mean(values * values, axis=-1, keepdims=True) + EPS) * gain


def on_device(
    tokens,
    attn_gain,
    w_query,
    w_key,
    w_value,
    mix_lambda,
    head_gain,
    w_output,
    cache_keys,
    cache_value,
    lengths,
    moe_gain,
    group_ids,
    member_ids,
    group_gate,
    member_logits,
    w_exp_gate,
    w_exp_up,
    w_exp_down,
):
    seqs, width = tokens.shape
    resid_in = tokens.astype(jnp.float32)
    normed = rms_scale(resid_in, attn_gain).astype(jnp.bfloat16)
    heads_local = mix_lambda.shape[0]
    qk_cols = w_query.shape[1]
    head_dim = qk_cols // (2 * heads_local)
    stacked = jnp.concatenate([w_query, w_key, w_value], axis=1)
    sliced = lax.all_to_all(normed, "ep", split_axis=1, concat_axis=0, tiled=True)
    projected = lax.psum_scatter(
        jnp.dot(sliced, stacked, preferred_element_type=jnp.float32),
        "ep",
        scatter_dimension=0,
        tiled=True,
    )
    projected = projected.astype(jnp.bfloat16)
    query = projected[:, :qk_cols]
    fresh_keys = projected[:, qk_cols : 2 * qk_cols]
    fresh_value = projected[:, 2 * qk_cols :]
    positions_all = cache_keys.shape[1]
    total_heads = heads_local * lax.axis_size("tp")
    head_index = (lax.axis_index("tp") * heads_local + jnp.arange(heads_local)).astype(jnp.float32)
    slopes = 2.0 ** (-8.0 * (head_index + 1.0) / total_heads)
    scale = head_dim ** (-0.5)
    positions = jnp.arange(positions_all)
    dist = (lengths[:, None] - positions[None, :]).astype(jnp.float32)
    valid = positions[None, :] < lengths[:, None]
    query4 = query.reshape(seqs, heads_local, 2, head_dim)
    keys5 = cache_keys.reshape(seqs, positions_all, heads_local, 2, head_dim)
    old = jnp.einsum("shcd,slhcd->cshl", query4, keys5, preferred_element_type=jnp.float32) * scale
    old = old - slopes[None, None, :, None] * dist[None, :, None, :]
    old = jnp.where(valid[None, :, None, :], old, -jnp.inf)
    fresh4 = fresh_keys.reshape(seqs, heads_local, 2, head_dim).astype(jnp.float32)
    new = jnp.moveaxis(jnp.sum(query4.astype(jnp.float32) * fresh4, axis=-1) * scale, 2, 0)
    full = jnp.concatenate([old, new[..., None]], axis=-1)
    maps = jax.nn.softmax(full, axis=-1)
    weights = (maps[0] - mix_lambda[None, :, None] * maps[1]).astype(jnp.bfloat16)
    values = cache_value.reshape(seqs, positions_all, heads_local, 2 * head_dim)
    head_mix = jnp.einsum(
        "shl,slhe->she", weights[..., :positions_all], values, preferred_element_type=jnp.float32
    )
    head_mix = head_mix + weights[..., positions_all].astype(jnp.float32)[
        ..., None
    ] * fresh_value.reshape(seqs, heads_local, 2 * head_dim).astype(jnp.float32)
    head_out = (
        rms_scale(head_mix, head_gain)
        .astype(jnp.bfloat16)
        .reshape(seqs, heads_local * 2 * head_dim)
    )
    term = jnp.dot(head_out, w_output, preferred_element_type=jnp.float32).astype(jnp.bfloat16)
    attn_sum = lax.psum(
        lax.optimization_barrier(term).astype(jnp.float32).astype(jnp.bfloat16), "tp"
    ).astype(jnp.float32)
    resid = resid_in + attn_sum
    moe_in = rms_scale(resid, moe_gain).astype(jnp.bfloat16)
    top = member_ids.shape[1]
    experts_local = w_exp_gate.shape[0]
    ep_count = lax.axis_size("ep")
    experts_all = experts_local * ep_count
    capacity = seqs * top // experts_all
    expert_ids = group_ids[:, None] * EPG + member_ids
    route_weight = jax.nn.softmax(member_logits, axis=-1) * group_gate[:, None]
    flat_ids = expert_ids.reshape(seqs * top)
    onehot = (flat_ids[:, None] == jnp.arange(experts_all)[None, :]).astype(jnp.int32)
    ranks = jnp.sum(jnp.cumsum(onehot, axis=0) * onehot, axis=1) - 1
    slot_grid = (flat_ids * capacity + ranks).reshape(seqs, top)
    slot_range = jnp.arange(experts_all * capacity)
    picker = jnp.sum((slot_grid[None, :, :] == slot_range[:, None, None]).astype(jnp.int32), axis=2)
    dispatch = jnp.dot(
        picker.astype(jnp.bfloat16), moe_in, preferred_element_type=jnp.float32
    ).astype(jnp.bfloat16)
    dispatch = dispatch.reshape(ep_count, experts_local, capacity, width)
    received = lax.all_to_all(dispatch, "ep", split_axis=0, concat_axis=2, tiled=True)
    received = received.reshape(experts_local, ep_count * capacity, width)
    gate = jnp.einsum("erd,edf->erf", received, w_exp_gate, preferred_element_type=jnp.float32)
    upper = jnp.einsum("erd,edf->erf", received, w_exp_up, preferred_element_type=jnp.float32)
    hidden = (jax.nn.silu(gate) * upper).astype(jnp.bfloat16)
    down = jnp.einsum("erf,efd->erd", hidden, w_exp_down, preferred_element_type=jnp.float32)
    summed = lax.psum_scatter(down.astype(jnp.bfloat16), "tp", scatter_dimension=2, tiled=True)
    cols = summed.shape[2]
    returned = lax.all_to_all(
        summed.reshape(experts_local, ep_count, capacity, cols),
        "ep",
        split_axis=1,
        concat_axis=0,
        tiled=True,
    )
    returned = returned.reshape(experts_all * capacity, cols)
    picked = returned[slot_grid].astype(jnp.float32)
    routed = jnp.sum(picked * route_weight[:, :, None], axis=1)
    own = lax.dynamic_slice_in_dim(resid, lax.axis_index("tp") * cols, cols, 1)
    mixed = (own + routed).astype(jnp.bfloat16)
    return (mixed, fresh_keys, fresh_value)


def solution(mesh):
    return jax.shard_map(
        on_device,
        mesh=mesh,
        in_specs=(
            P("ep", None),
            P(),
            P("ep", "tp"),
            P("ep", "tp"),
            P("ep", "tp"),
            P("tp"),
            P(),
            P("tp", None),
            P("ep", None, "tp"),
            P("ep", None, "tp"),
            P("ep"),
            P(),
            P("ep"),
            P("ep", None),
            P("ep"),
            P("ep", None),
            P("ep", None, "tp"),
            P("ep", None, "tp"),
            P("ep", "tp", None),
        ),
        out_specs=(P("ep", "tp"), P("ep", "tp"), P("ep", "tp")),
        check_vma=False,
    )
```

profile of v0, /device:TPU:0, one launch (start us, length us, event | category | flops | bytes accessed | tf_op | source)
XLA Modules:
  0.0 177.5 jit_solution(10258000634573673739)
XLA Ops:
  7.2 1.2 fusion.27
  8.4 1.0 fusion.29
  9.4 0.6 copy.110
  10.0 5.2 %all-to-all-start = ((bf16[16,4,1024]{2,0,1:T(8,128)(2,1)}), bf16[16,4,1024]{2,0,1:T(8,128)(2,1)S(1)}, u32[]{:S(2)}, u32[]{:S(2)}) async-start(bf16[16,4,1024]{2,0,1:T(8,128)(2,1)} %bitcast.80), calls=%async_computation | async-start | bytes 262144 | tf_op jit(solution)/shard_map/all_to_all | solution.py:44
  15.2 0.7 subtract_convert_fusion
  16.0 0.8 copy.78
  16.7 0.7 broadcast_multiply_fusion.1
  17.7 0.2 select_reduce_fusion
  18.0 2.2 %all-to-all-done = bf16[16,4,1024]{2,0,1:T(8,128)(2,1)S(1)} async-done(((bf16[16,4,1024]{2,0,1:T(8,128)(2,1)}), bf16[16,4,1024]{2,0,1:T(8,128)(2,1)S(1)}, u32[]{:S(2)}, u32[]{:S(2)}) %all-to-all-start) | async-done | bytes 131104 | tf_op jit(solution)/shard_map/all_to_all | solution.py:44
  20.3 2.5 %fusion.12 = f32[64,768]{1,0:T(8,128)} fusion(bf16[64,1024]{1,0:T(8,128)(2,1)S(1)} %bitcast.84, bf16[1024,256]{1,0:T(8,128)(2,1)} %param.23, bf16[1024,256]{1,0:T(8,128)(2,1)} %param.22, bf16[1024,256]{1,0:T(8,128)(2,1)} %param.21), kind=kOutput, calls=%fused_computation.16 | convolution fusion | flops 105381888 | bytes 1900544 | tf_op jit(solution)/shard_map/dot_general | solution.py:46
  22.9 12.3 %copy.74 = bf16[16,1024,256]{1,2,0:T(8,128)(2,1)} copy(bf16[16,1024,256]{2,1,0:T(8,128)(2,1)} %param.27) | data formatting | bytes 16777216 | tf_op args[8]
  35.4 11.5 %reduce-scatter.3.cloned.1.call-done = f32[16,768]{1,0:T(8,128)} async-done(((f32[64,768]{1,0:T(8,128)}), f32[16,768]{1,0:T(8,128)}) %reduce-scatter.3.cloned.1.call-update) | async-done | bytes 49168 | tf_op jit(solution)/shard_map/reduce_scatter | solution.py:45
  46.9 0.8 convert_element_type.87
  48.2 4.6 %fusion.3 = f32[2,16,2,1,1024]{4,3,2,1,0:T(1,128)S(1)} fusion(bf16[16,1024,2,2,64]{1,4,3,2,0:T(8,128)(2,1)} %bitcast.81, bf16[16,2,2,64,1]{3,2,1,0,4:T(2,128)(2,1)S(1)} %reshape.201), kind=kOutput, calls=%fused_computation.4 | convolution fusion | flops 8388608 | bytes 8658944 | tf_op jit(solution)/shard_map/shcd,slhcd->cshl/dot_general | solution.py:65
  52.8 0.2 fusion.66
  53.1 0.8 fusion.35
  54.1 0.2 copy.89
  54.3 4.7 %fusion = f32[16,2,1,128]{3,2,1,0:T(1,128)S(1)} fusion(bf16[16,2,1024,1]{2,0,1,3:T(8,128)(2,1)S(1)} %slice_bitcast_fusion.2, bf16[16,1024,256]{2,1,0:T(8,128)(2,1)} %param.28), kind=kOutput, calls=%fused_computation.1 | convolution fusion | flops 8388608 | bytes 8470528 | tf_op jit(solution)/shard_map/shl,slhe->she/dot_general | solution.py:74
  59.0 0.2 multiply_reduce_fusion.3
  59.3 1.0 convolution_convert_fusion.2
  60.5 55.0 %all-reduce.2.cloned.1.call-done = bf16[16,4096]{1,0:T(8,128)(2,1)} async-done(((bf16[16,4096]{1,0:T(8,128)(2,1)}), bf16[16,4096]{1,0:T(8,128)(2,1)}) %all-reduce.2.cloned.1.call-update) | async-done | bytes 131088 | tf_op jit(solution)/shard_map/psum | solution.py:86
  115.5 1.1 convert_add_fusion
  116.6 1.2 fusion.5
  117.8 9.2 %all_to_all.37 = bf16[4,1,8,4096]{3,2,1,0:T(8,128)(2,1)S(1)} all-to-all(bf16[4,1,8,4096]{3,2,1,0:T(8,128)(2,1)S(1)} %fusion.5), channel_id=1, replica_groups=mesh['ep'=4,'tp'=8] {'ep'}, dimensions={0} | all-to-all | bytes 524288 | tf_op jit(solution)/shard_map/all_to_all | solution.py:108
  126.9 2.0 %fusion.10 = f32[32,256]{1,0:T(8,128)S(1)} fusion(bf16[1,4096,256]{2,1,0:T(8,128)(2,1)} %param.35, bf16[4,1,8,4096]{3,2,1,0:T(8,128)(2,1)S(1)} %all_to_all.37), kind=kOutput, calls=%fused_computation.14 | convolution fusion | flops 67108864 | bytes 2392064 | tf_op jit(solution)/shard_map/erd,edf->erf/dot_general | solution.py:110
  129.0 3.6 %fusion.6 = bf16[1,32,4096]{2,1,0:T(8,128)(2,1)} fusion(bf16[1,256,4096]{2,1,0:T(8,128)(2,1)S(1)} %copy-done, bf16[1,4096,256]{2,1,0:T(8,128)(2,1)} %param.36, bf16[4,1,8,4096]{3,2,1,0:T(8,128)(2,1)S(1)} %all_to_all.37, f32[32,256]{1,0:T(8,128)S(1)} %fusion.10), kind=kOutput, calls=%fused_computation.9 | convolution fusion | flops 134397952 | bytes 4751360 | tf_op jit(solution)/shard_map/erf,efd->erd/dot_general | solution.py:113
  132.8 28.4 %reduce-scatter.5.cloned.1.call-done = bf16[1,32,512]{2,1,0:T(8,128)(2,1)} async-done(((bf16[1,32,4096]{2,1,0:T(8,128)(2,1)}), bf16[1,32,512]{2,1,0:T(8,128)(2,1)}) %reduce-scatter.5.cloned.1.call-update) | async-done | bytes 32784 | tf_op jit(solution)/shard_map/reduce_scatter | solution.py:114
  161.1 3.7 %all-to-all-start.2 = ((bf16[1,4,8,512]{3,2,0,1:T(8,128)(2,1)}), bf16[1,4,8,512]{3,2,0,1:T(8,128)(2,1)S(1)}, u32[]{:S(2)}, u32[]{:S(2)}) async-start(bf16[1,4,8,512]{3,2,0,1:T(8,128)(2,1)} %bitcast.90), calls=%async_computation.4 | async-start | bytes 65536 | tf_op jit(solution)/shard_map/all_to_all | solution.py:116
  164.9 4.7 %all-to-all-done.2 = bf16[1,4,8,512]{3,2,0,1:T(8,128)(2,1)S(1)} async-done(((bf16[1,4,8,512]{3,2,0,1:T(8,128)(2,1)}), bf16[1,4,8,512]{3,2,0,1:T(8,128)(2,1)S(1)}, u32[]{:S(2)}, u32[]{:S(2)}) %all-to-all-start.2) | async-done | bytes 32800 | tf_op jit(solution)/shard_map/all_to_all | solution.py:116
  169.5 0.6 gather_fusion
  170.2 0.1 multiply_reduce_fusion.1
  170.4 0.6 add_convert_fusion
  (64 shorter events, 2.1 us)
Async XLA Ops:
  7.2 121.8 %copy-start = (bf16[1,256,4096]{2,1,0:T(8,128)(2,1)S(1)}, bf16[1,256,4096]{2,1,0:T(8,128)(2,1)}, u32[]{:S(2)}) copy-start(bf16[1,256,4096]{2,1,0:T(8,128)(2,1)} %param.37) | copy-start | bytes 6291460
  10.0 10.2 %all-to-all-start = ((bf16[16,4,1024]{2,0,1:T(8,128)(2,1)}), bf16[16,4,1024]{2,0,1:T(8,128)(2,1)S(1)}, u32[]{:S(2)}, u32[]{:S(2)}) async-start(bf16[16,4,1024]{2,0,1:T(8,128)(2,1)} %bitcast.80), calls=%async_computation | async-start | bytes 262144 | tf_op jit(solution)/shard_map/all_to_all | solution.py:44
  15.2 31.7 %reduce-scatter.3.cloned.1.call-start = ((), (), s32[]{:S(2)}) async-start(), calls=%async_computation.5 | async-start | bytes 245760 | tf_op jit(solution)/shard_map/reduce_scatter | solution.py:45
  20.3 2.6 %copy-start.7 = (s32[16]{0:T(128)S(1)}, s32[16]{0:T(128)}, u32[]{:S(2)}) copy-start(s32[16]{0:T(128)} %param.29) | copy-start | bytes 196
  22.8 92.7 %all-reduce.2.cloned.1.call-start = ((), (), s32[]{:S(2)}) async-start(), calls=%async_computation.6 | async-start | bytes 262144 | tf_op jit(solution)/shard_map/psum | solution.py:86
  47.7 5.1 %copy-start.4 = (bf16[16,256]{1,0:T(8,128)(2,1)}, bf16[16,256]{1,0:T(8,128)(2,1)S(1)}, u32[]{:S(2)}) copy-start(bf16[16,256]{1,0:T(8,128)(2,1)S(1)} %get-tuple-element.10) | copy-start | bytes 24580
  47.7 6.5 %copy-start.3 = (bf16[16,256]{1,0:T(8,128)(2,1)}, bf16[16,256]{1,0:T(8,128)(2,1)S(1)}, u32[]{:S(2)}) copy-start(bf16[16,256]{1,0:T(8,128)(2,1)S(1)} %get-tuple-element.9) | copy-start | bytes 24580
  52.8 1.1 copy-start.8
  54.3 4.9 %copy-start.9 = (f32[128]{0:T(128)S(1)}, f32[128]{0:T(128)}, u32[]{:S(2)}) copy-start(f32[128]{0:T(128)} %param.25) | copy-start | bytes 1540
  54.3 5.0 %copy-start.2 = (bf16[256,4096]{1,0:T(8,128)(2,1)S(1)}, bf16[256,4096]{1,0:T(8,128)(2,1)}, u32[]{:S(2)}) copy-start(bf16[256,4096]{1,0:T(8,128)(2,1)} %param.26) | copy-start | bytes 6291460
  59.0 56.5 %copy-start.1 = (bf16[16,4096]{1,0:T(8,128)(2,1)S(1)}, bf16[16,4096]{1,0:T(8,128)(2,1)}, u32[]{:S(2)}) copy-start(bf16[16,4096]{1,0:T(8,128)(2,1)} %param.19) | copy-start | bytes 393220
  59.0 57.5 %copy-start.5 = (f32[4096]{0:T(1024)S(1)}, f32[4096]{0:T(1024)}, u32[]{:S(2)}) copy-start(f32[4096]{0:T(1024)} %param.30) | copy-start | bytes 49156
  60.4 100.7 %reduce-scatter.5.cloned.1.call-start = ((), (), s32[]{:S(2)}) async-start(), calls=%async_computation.7 | async-start | bytes 294912 | tf_op jit(solution)/shard_map/reduce_scatter | solution.py:114
  129.0 3.7 %copy-start.6 = (f32[16,2]{0,1:T(2,128)S(1)}, f32[16,2]{0,1:T(2,128)}, u32[]{:S(2)}) copy-start(f32[16,2]{0,1:T(2,128)} %param.34) | copy-start | bytes 388
  129.0 3.8 %copy-start.10 = (f32[16]{0:T(128)S(1)}, f32[16]{0:T(128)}, u32[]{:S(2)}) copy-start(f32[16]{0:T(128)} %param.33) | copy-start | bytes 196
  161.1 8.4 %all-to-all-start.2 = ((bf16[1,4,8,512]{3,2,0,1:T(8,128)(2,1)}), bf16[1,4,8,512]{3,2,0,1:T(8,128)(2,1)S(1)}, u32[]{:S(2)}, u32[]{:S(2)}) async-start(bf16[1,4,8,512]{3,2,0,1:T(8,128)(2,1)} %bitcast.90), calls=%async_computation.4 | async-start | bytes 65536 | tf_op jit(solution)/shard_map/all_to_all | solution.py:116
Sparse Core Ops, SparseCore 0:
  22.9 23.9 reduce-scatter.2
  60.5 54.9 all-reduce.1
  132.7 28.3 reduce-scatter.4
where the time goes:
time: 178 us
  waiting for transfers between devices  102 us (57%)
  matrix products  19.6 us (11%)
  local copies, waits for them, and re-layouts  15.5 us (9%)
  between operations  14 us (8%)
  blocking collectives  9.17 us (5%)
  starting transfers between devices  8.93 us (5%)
  other arithmetic  8.5 us (5%)
    psum x1, waiting for transfers between devices, on_device(): lax.psum(lax.optimization_barrier(term).astype(jnp.float32).astype(jnp.bf...  55 us
    reduce_scatter x1, waiting for transfers between devices, on_device(): lax.psum_scatter(down.astype(jnp.bfloat16), 'tp', scatter_dimension=2, ti...  28.4 us
    unnamed x24, local copies, waits for them, and re-layouts  13.1 us
    reduce_scatter x1, waiting for transfers between devices, on_device(): lax.psum_scatter(jnp.dot(sliced, stacked, preferred_element_type=jnp.floa...  11.5 us
    all_to_all x1, blocking collectives, on_device(): lax.all_to_all(dispatch, 'ep', split_axis=0, concat_axis=2, tiled=True)  9.17 us
    all_to_all x1, starting transfers between devices, on_device(): lax.all_to_all(normed, 'ep', split_axis=1, concat_axis=0, tiled=True)  5.19 us
    dot_general x1, matrix products, on_device(): jnp.einsum('shl,slhe->she', weights[..., :positions_all], values, preferr...  4.72 us
    all_to_all x1, waiting for transfers between devices, on_device(): lax.all_to_all(summed.reshape(experts_local, ep_count, capacity, cols), '...  4.66 us
  transfers between devices with their start and end apart: 5, of which 5 were waited for; matrix products, arithmetic and copies ran while one was open for 9% of the time, Pallas kernels for 0%

commit v1 on v0

v1 whole, which is shorter than its diff:
```python
import functools
import itertools

import jax
import jax.numpy as jnp
from jax import lax
from jax.experimental import pallas as pl
from jax.experimental.pallas import tpu as pltpu
from jax.sharding import PartitionSpec as P

EPG = 2
EPS = 1e-06
F32, BF16 = jnp.float32, jnp.bfloat16
LANES, SUB = 128, 8
CORES = 2
VMEM = pl.BlockSpec(memory_space=pltpu.VMEM)
HBM = pl.BlockSpec(memory_space=pltpu.HBM)
ANY = pl.BlockSpec(memory_space=pl.ANY)


def params(mib):
    return pltpu.CompilerParams(vmem_limit_bytes=mib << 20)


def cost(flops):
    return pl.CostEstimate(flops=int(flops), bytes_accessed=1 << 20, transcendentals=0)


def dot(a, b):
    return jnp.dot(a, b, preferred_element_type=F32)


def slabs(width, n_tp, parity):
    slab = width // n_tp
    for z in range(n_tp // CORES):
        start = (z * CORES + parity) * slab
        yield z, slice(z * slab, (z + 1) * slab), pl.ds(pl.multiple_of(start, LANES), slab)


def slices_kernel(tokens_hbm, gain_hbm, *refs):
    *outs, tokens, gain, sems = refs
    n = len(outs)
    seqs, width = tokens.shape
    cols = width // n
    copies = [pltpu.make_async_copy(gain_hbm, gain, sems.at[n])]
    for k in range(n):
        at = slice(k * cols, (k + 1) * cols)
        copies.append(pltpu.make_async_copy(tokens_hbm.at[:, at], tokens.at[:, at], sems.at[k]))
    for copy in copies:
        copy.start()
    for copy in copies:
        copy.wait()
    x = tokens[...].astype(F32)
    scale = lax.rsqrt(jnp.sum(x * x, axis=1, keepdims=True) * (1.0 / width) + EPS)
    for k, out in enumerate(outs):
        at = pl.ds(pl.multiple_of((lax.axis_index("ep") ^ k) * cols, LANES), cols)
        out[...] = (tokens[:, at].astype(F32) * scale * gain[:, at]).astype(BF16)


def tables_kernel(groups, group_ids, member_ids, logits, gate, picker, picks, shares):
    top, seqs = member_ids.shape
    cap = seqs // groups
    row = lax.broadcasted_iota(jnp.int32, (seqs, seqs), 0)
    col = lax.broadcasted_iota(jnp.int32, (seqs, seqs), 1)

    def column(line):
        return jnp.sum(jnp.where(row == col, line, 0.0), axis=1, keepdims=True)

    group = group_ids[...].astype(F32)
    same = column(group) == group
    rank_line = jnp.sum(jnp.where(same & (row < col), 1.0, 0.0), axis=0, keepdims=True)
    rank = jnp.sum(jnp.where(same & (col < row), 1.0, 0.0), axis=1, keepdims=True)
    spot = lax.broadcasted_iota(jnp.int32, picker.shape, 0)
    wanted = ((lax.axis_index("ep") ^ (spot // cap)) // EPG).astype(F32)
    here = (group == wanted) & (rank_line == (spot % cap).astype(F32))
    picker[...] = here.astype(F32).astype(BF16)
    route = jnp.exp(logits[...] - jnp.max(logits[...], axis=0, keepdims=True))
    route = route / jnp.sum(route, axis=0, keepdims=True) * gate[...]
    spot = lax.broadcasted_iota(jnp.int32, (seqs, picks.shape[1]), 1).astype(F32)
    for k in range(top):
        expert = column(group * EPG + member_ids[k : k + 1, :].astype(F32))
        picks[k * seqs : (k + 1) * seqs, :] = (expert * cap + rank == spot).astype(F32).astype(BF16)
        shares[k * seqs : (k + 1) * seqs, :] = jnp.broadcast_to(column(route[k : k + 1]), (seqs, LANES))


def project_kernel(n, *refs):
    ins, weights, outs = refs[:n], refs[n : n + 3], refs[n + 4 :]
    seqs = ins[0].shape[0]
    rows = jnp.concatenate([ref[...] for ref in ins], axis=0)
    for j, weight in enumerate(weights):
        cols = weight.shape[1]
        got = dot(rows, weight[...])
        for k, out in enumerate(outs):
            out[:, j * cols : (j + 1) * cols] = got[k * seqs : (k + 1) * seqs]


def attention_kernel(n, total_heads, lengths, lam, *refs):
    parts = refs[:n]
    head_gain, keys, values, w_out, mine, theirs, fresh_k, fresh_v, spread, scores, fresh_share, *mixed = refs[n:]
    seqs, spots, cols = keys.shape
    width = w_out.shape[1]
    heads = lam.shape[1]
    wide = cols // heads
    head_dim = wide // 2
    maps = 2 * heads
    used = maps * seqs
    per = SUB // maps
    total = parts[0][...]
    for part in parts[1:]:
        total = total + part[...]
    projected = total.astype(BF16)
    query, fresh, value = (projected[:, j * cols : (j + 1) * cols] for j in range(3))
    fresh_k[...] = fresh
    fresh_v[...] = value
    repeat = lax.broadcasted_iota(jnp.int32, (used, seqs), 0) // maps
    repeat = (repeat == lax.broadcasted_iota(jnp.int32, (used, seqs), 1)).astype(F32).astype(BF16)
    row = lax.broadcasted_iota(jnp.int32, (used, cols), 0)
    col = lax.broadcasted_iota(jnp.int32, (used, cols), 1)
    query = jnp.where(row % maps == col // head_dim, dot(repeat, query), 0.0)
    spread[...] = query
    factor = head_dim ** (-0.5)
    new = jnp.sum(query * dot(repeat, fresh), axis=1, keepdims=True) * factor
    inside = lax.broadcasted_iota(jnp.int32, (SUB, 1), 0) // maps

    def one_score(i, carry):
        at = pl.ds(pl.multiple_of(i * SUB, SUB), SUB)
        block, got = spread[at, :], 0.0
        for p in range(per):
            lhs = jnp.where(inside == p, block, 0.0).astype(BF16)
            got += lax.dot_general(lhs, keys[i * per + p], (((1,), (1,)), ((), ())), preferred_element_type=F32)
        scores[at, :] = got
        return carry

    lax.fori_loop(0, used // SUB, one_score, 0, unroll=True)
    line = lax.broadcasted_iota(jnp.int32, (used, LANES), 0)
    whose = line[:, :seqs] // maps == lax.broadcasted_iota(jnp.int32, (used, seqs), 1)
    count = jnp.sum(jnp.where(whose, lengths[...].astype(F32), 0.0), axis=1, keepdims=True)
    head = (lax.axis_index("tp") * heads + (line % maps) // 2).astype(F32)
    slope = jnp.exp2(-8.0 * (head + 1.0) / total_heads)
    mix = jnp.zeros((used, LANES), F32)
    for h in range(heads):
        mix = jnp.where((line % maps) // 2 == h, lam[:, h : h + 1], mix)
    pieces = []
    top = jnp.broadcast_to(new, (used, LANES))
    for at in range(0, spots, LANES):
        spot = (lax.broadcasted_iota(jnp.int32, (used, LANES), 1) + at).astype(F32)
        piece = scores[:, at : at + LANES] * factor - slope * (count - spot)
        piece = jnp.where(spot < count, piece, -jnp.inf)
        pieces.append(piece)
        top = jnp.maximum(top, piece)
    top = jnp.max(top, axis=1, keepdims=True)
    new = jnp.exp(new - top)
    pieces = [jnp.exp(piece - top) for piece in pieces]
    norm = 1.0 / (jnp.sum(functools.reduce(jnp.add, pieces), axis=1, keepdims=True) + new)

    def blend(piece):
        piece = piece * norm
        return piece - mix * pltpu.roll(piece, used - 1, 0)

    for j, piece in enumerate(pieces):
        scores[:, j * LANES : (j + 1) * LANES] = blend(piece)
    fresh_share[...] = blend(jnp.broadcast_to(new, (used, LANES)))

    def one_mix(i, carry):
        at = pl.ds(pl.multiple_of(i * SUB, SUB), SUB)
        block, got = scores[at, :], 0.0
        for p in range(per):
            lhs = jnp.where(inside == p, block, 0.0).astype(BF16)
            got += dot(lhs, values[i * per + p])
        for h in range(heads):
            mixed[h][at, :] = got[:, h * wide : (h + 1) * wide]
        return carry

    lax.fori_loop(0, used // SUB, one_mix, 0, unroll=True)
    outs = []
    for h in range(heads):
        at = slice(h * wide, (h + 1) * wide)
        rows = pl.ds(2 * h, seqs, stride=maps)
        share = fresh_share[rows, :].astype(BF16).astype(F32)
        both = mixed[h][rows, :] + share * value[:, at].astype(F32)
        mean = jnp.mean(both * both, axis=1, keepdims=True)
        outs.append((both * lax.rsqrt(mean + EPS) * head_gain[...]).astype(BF16))
    out = jnp.concatenate(outs, axis=1)
    first = lax.axis_index("tp") % CORES == 0
    slab = width * heads // total_heads
    for z in range(mine.shape[1] // slab):
        at, start = slice(z * slab, (z + 1) * slab), z * CORES * slab
        even, odd = (dot(out, w_out[:, lo : lo + slab]) for lo in (start, start + slab))
        mine[:, at] = jnp.where(first, even, odd).astype(BF16)
        theirs[:, at] = jnp.where(first, odd, even).astype(BF16)


def pair_kernel(mine, got, out):
    out[...] = (mine[...].astype(F32) + got[...].astype(F32)).astype(BF16)


def dispatch_kernel(n_ep, n_tp, n, picker, tokens, *refs):
    parts, resid, outs = refs[:n], refs[n], refs[n + 1 :]
    cap = outs[0].shape[0]
    index = lax.axis_index("tp")
    own = jnp.zeros(resid.shape, F32)
    for z, at, cut in slabs(tokens.shape[1], n_tp, index % CORES):
        total = parts[0][:, at].astype(F32)
        for part in parts[1:]:
            total = total + part[:, at].astype(F32)
        total = tokens[:, cut].astype(F32) + total
        own = jnp.where(index // CORES == z, total, own)
        rows = dot(picker[...], total.astype(BF16)).astype(BF16)
        for k, out in enumerate(outs):
            out[:, at] = rows[k * cap : (k + 1) * cap]
    resid[...] = own


def stack_kernel(*refs):
    for k, ref in enumerate(refs[:-1]):
        cap = ref.shape[0]
        refs[-1][k * cap : (k + 1) * cap, :] = ref[...]


def expert_kernel(n_ep, n_tp, mine, theirs, gain, w_gate, w_up, w_down, back):
    slab = back.shape[2]
    cap = back.shape[1] // n_tp
    width = slab * n_tp
    core = lax.axis_index("tp") % CORES
    blocks = []
    for head, tail, parity in ((mine, theirs, core), (theirs, mine, 1 - core)):
        for _, at, cut in slabs(width, n_tp, parity):
            blocks.append((cut, jnp.concatenate([head[:cap, at].astype(F32), tail[cap:, at].astype(F32)], axis=0)))
    square = sum(jnp.sum(x * x, axis=1, keepdims=True) for _, x in blocks)
    scale = lax.rsqrt(square * (1.0 / width) + EPS)
    gate, upper = 0.0, 0.0
    for cut, x in blocks:
        x = (x * scale * gain[:, cut]).astype(BF16)
        gate += dot(x, w_gate[0, cut, :])
        upper += dot(x, w_up[0, cut, :])
    hidden = (gate * (1.0 / (1.0 + jnp.exp(-gate))) * upper).astype(BF16)
    for t in range(n_tp):
        down = dot(hidden, w_down[0, :, t * slab : (t + 1) * slab]).astype(BF16)
        for k in range(n_ep):
            back[lax.axis_index("ep") ^ k, t * cap : (t + 1) * cap, :] = down[k * cap : (k + 1) * cap]


def combine_kernel(n_ep, n_tp, back, resid, picks, shares, mixed):
    seqs, slab = resid.shape
    cap = back.shape[0] // (n_ep * n_tp)
    outs = []
    for e in range(n_ep):
        total = jnp.zeros((cap, slab), F32)
        for t in range(n_tp):
            lo = (e * n_tp + t) * cap
            total = total + back[lo : lo + cap, :].astype(F32)
        outs.append(total)
    picked = dot(picks[...], jnp.concatenate(outs, axis=0).astype(BF16))
    total = resid[...]
    for k in range(picked.shape[0] // seqs):
        lines = slice(k * seqs, (k + 1) * seqs)
        total = total + shares[lines, :1] * picked[lines]
    mixed[...] = total.astype(BF16)


def on_device(
    n_ep, n_tp,
    tokens, attn_gain, w_query, w_key, w_value, mix_lambda, head_gain, w_output, cache_keys, cache_value, lengths,
    moe_gain, group_ids, member_ids, group_gate, member_logits, w_exp_gate, w_exp_up, w_exp_down,
):
    seqs, width = tokens.shape
    cols = w_query.shape[1]
    slab = width // n_tp
    groups = n_ep * w_exp_gate.shape[0] // EPG
    heads = mix_lambda.shape[0]
    shape = jax.ShapeDtypeStruct

    def send(piece, axis, count, k):
        return lax.ppermute(piece, axis, [(i, i ^ k) for i in range(count)])

    def swap(pieces):
        return [pieces[0]] + [send(piece, "ep", n_ep, k) for k, piece in enumerate(pieces) if k]

    def cross(pieces):
        pairs = itertools.product(range(n_ep), range(n_tp))
        pairs = [(e, t, e * n_tp + t) for e, t in pairs]
        return [pieces[0]] + [
            lax.ppermute(piece, ("ep", "tp"), [(i, (e ^ k) * n_tp + (t ^ 1)) for e, t, i in pairs])
            for k, piece in enumerate(pieces)
            if k
        ]

    slices = pl.pallas_call(
        slices_kernel,
        out_shape=[shape((seqs, width // n_ep), BF16)] * n_ep,
        in_specs=[HBM] * 2,
        out_specs=[VMEM] * n_ep,
        scratch_shapes=[
            pltpu.VMEM((seqs, width), BF16),
            pltpu.VMEM((1, width), F32),
            pltpu.SemaphoreType.DMA((n_ep + 1,)),
        ],
        compiler_params=params(2),
        cost_estimate=cost(2e10),
        name="slices",
    )(*(pltpu.with_memory_space_constraint(x, pltpu.HBM) for x in (tokens, attn_gain.reshape(1, width))))
    pairs = n_ep * n_tp * (seqs // groups)
    top = member_ids.shape[1]
    picker, picks, shares = pl.pallas_call(
        functools.partial(tables_kernel, groups),
        out_shape=[shape((pairs // n_tp, seqs), BF16), shape((top * seqs, pairs // n_tp), BF16), shape((top * seqs, LANES), F32)],
        in_specs=[VMEM] * 4,
        out_specs=[VMEM] * 3,
        compiler_params=params(2),
        cost_estimate=cost(1e9),
        name="tables",
    )(group_ids.reshape(1, seqs), member_ids.T, member_logits.T, group_gate.reshape(1, seqs))
    parts = pl.pallas_call(
        functools.partial(project_kernel, n_ep),
        out_shape=[shape((seqs, 3 * cols), F32)] * n_ep,
        in_specs=[VMEM] * (n_ep + 3) + [ANY],
        out_specs=[VMEM] * n_ep,
        compiler_params=params(6),
        cost_estimate=cost(2e10),
        name="project",
    )(*cross(slices), w_query, w_key, w_value, shares)
    mine, theirs, fresh_keys, fresh_value = pl.pallas_call(
        functools.partial(attention_kernel, n_ep, heads * n_tp),
        out_shape=[shape((seqs, width // CORES), BF16)] * 2 + [shape((seqs, cols), BF16)] * 2,
        in_specs=[VMEM] * (n_ep + 6),
        out_specs=[VMEM] * 4,
        scratch_shapes=[
            pltpu.VMEM((2 * heads * seqs, cols), F32),
            pltpu.VMEM((2 * heads * seqs, cache_keys.shape[1]), F32),
        ]
        + [pltpu.VMEM((2 * heads * seqs, LANES), F32)] * (1 + heads),
        compiler_params=params(6),
        cost_estimate=cost(1e10),
        name="attention",
    )(
        lengths.reshape(1, seqs), mix_lambda.reshape(1, heads), *swap(parts), head_gain.reshape(1, -1),
        cache_keys, cache_value, w_output,
    )
    pair = pl.pallas_call(
        pair_kernel,
        out_shape=shape(mine.shape, BF16),
        in_specs=[VMEM] * 2,
        out_specs=VMEM,
        compiler_params=params(2),
        cost_estimate=cost(5e8),
        name="pair",
    )(mine, send(theirs, "tp", n_tp, 1))
    halves = [pair] + [send(pair, "tp", n_tp, CORES * k) for k in range(1, n_tp // CORES)]
    cap = seqs // groups
    resid, *rows = pl.pallas_call(
        functools.partial(dispatch_kernel, n_ep, n_tp, len(halves)),
        out_shape=[shape((seqs, slab), F32)] + [shape((cap, width // CORES), BF16)] * n_ep,
        in_specs=[VMEM] * (2 + len(halves)),
        out_specs=[VMEM] * (1 + n_ep),
        compiler_params=params(2),
        cost_estimate=cost(5e9),
        name="dispatch",
    )(picker, tokens, *halves)
    mine = pl.pallas_call(
        stack_kernel,
        out_shape=shape((n_ep * cap, width // CORES), BF16),
        in_specs=[VMEM] * n_ep,
        out_specs=VMEM,
        compiler_params=params(2),
        cost_estimate=cost(5e8),
        name="stack",
    )(*cross(rows))
    back = pl.pallas_call(
        functools.partial(expert_kernel, n_ep, n_tp),
        out_shape=shape((n_ep, n_tp * cap, slab), BF16),
        in_specs=[VMEM] * 6,
        out_specs=VMEM,
        compiler_params=params(10),
        cost_estimate=cost(5e9),
        name="experts",
    )(mine, send(mine, "tp", n_tp, 1), moe_gain.reshape(1, width), w_exp_gate, w_exp_up, w_exp_down)
    back = back.reshape(pairs, slab)
    back = lax.all_to_all(back, ("ep", "tp"), split_axis=0, concat_axis=0, tiled=True)
    mixed = pl.pallas_call(
        functools.partial(combine_kernel, n_ep, n_tp),
        out_shape=shape((seqs, slab), BF16),
        in_specs=[VMEM] * 4,
        out_specs=VMEM,
        compiler_params=params(2),
        cost_estimate=cost(1e9),
        name="combine",
    )(back, resid, picks, shares)
    return mixed, fresh_keys, fresh_value


def solution(mesh):
    return jax.shard_map(
        functools.partial(on_device, mesh.shape["ep"], mesh.shape["tp"]),
        mesh=mesh,
        in_specs=(
            P("ep", None), P(), P("ep", "tp"), P("ep", "tp"), P("ep", "tp"), P("tp"), P(), P("tp", None),
            P("ep", None, "tp"), P("ep", None, "tp"), P("ep"), P(), P("ep"), P("ep", None), P("ep"), P("ep", None),
            P("ep", None, "tp"), P("ep", None, "tp"), P("ep", "tp", None),
        ),
        out_specs=(P("ep", "tp"), P("ep", "tp"), P("ep", "tp")),
        check_vma=False,
    )
```

time: 178 us -> 56.5 us (0.32)
  waiting for transfers between devices: 102 us -> 18.7 us
  matrix products: 19.6 us -> 0 us
  local copies, waits for them, and re-layouts: 15.5 us -> 0.12 us
  between operations: 14 us -> 0.92 us
  other arithmetic: 8.5 us -> 0.01 us
  Pallas kernels: 0 us -> 8.26 us
  starting transfers between devices: 8.93 us -> 15.5 us
  blocking collectives: 9.17 us -> 12.5 us
    psum x1 -> x0, waiting for transfers between devices: 55 us -> none  [on_device(): lax.psum(lax.optimization_barrier(term).astype(jnp.float32).astype(jnp.bf...]
    reduce_scatter x2 -> x0, waiting for transfers between devices: 39.9 us -> none  [the longest x1 28.4 us: on_device(): lax.psum_scatter(down.astype(jnp.bfloat16), 'tp', scatter_dimension=2, ti...]
    dot_general x7 -> x0, matrix products: 19.6 us -> none  [the longest x1 4.72 us: on_device(): jnp.einsum('shl,slhe->she', weights[..., :positions_all], values, preferr...]
    ppermute x0 -> x14, waiting for transfers between devices: none -> 18.7 us  [the longest x8 9.9 us: send(): return lax.ppermute(piece, axis, [(i, i ^ k) for i in range(count)])]
    ppermute x0 -> x14, starting transfers between devices: none -> 15.5 us  [the longest x8 8.31 us: send(): return lax.ppermute(piece, axis, [(i, i ^ k) for i in range(count)])]
    unnamed x24 -> x40, local copies, waits for them, and re-layouts: 13.1 us -> 0.12 us
    all_to_all x2 -> x0, starting transfers between devices: 8.84 us -> none  [the longest x1 5.19 us: on_device(): lax.all_to_all(normed, 'ep', split_axis=1, concat_axis=0, tiled=True)]
    pallas_call x0 -> x9, Pallas kernels: none -> 8.26 us  [the longest x1 4.37 us: on_device(): pl.pallas_call(functools.partial(attention_kernel, n_ep, heads * n_tp), o...]
  transfers between devices with their start and end apart: 5 -> 14, of which waited for: 5 -> 12; matrix products, arithmetic and copies ran while one was open for 9% -> 0% of each run, Pallas kernels for 0% -> 0%
where the time goes in v1:
time: 56.5 us; the launch traced here: 56.1 us
  waiting for transfers between devices  18.7 us (33%)
  starting transfers between devices  15.5 us (27%)
  blocking collectives  12.5 us (22%)
  Pallas kernels  8.26 us (15%)
  between operations  0.92 us (2%)
    all_to_all x1, blocking collectives, on_device(): lax.all_to_all(back, ('ep', 'tp'), split_axis=0, concat_axis=0, tiled=True)  12.5 us
    ppermute x8, waiting for transfers between devices, send(): return lax.ppermute(piece, axis, [(i, i ^ k) for i in range(count)])  9.9 us
    ppermute x6, waiting for transfers between devices, cross(): lax.ppermute(piece, ('ep', 'tp'), [(i, (e ^ k) * n_tp + (t ^ 1)) for e, t...  8.81 us
    ppermute x8, starting transfers between devices, send(): return lax.ppermute(piece, axis, [(i, i ^ k) for i in range(count)])  8.31 us
    ppermute x6, starting transfers between devices, cross(): lax.ppermute(piece, ('ep', 'tp'), [(i, (e ^ k) * n_tp + (t ^ 1)) for e, t...  7.19 us
    pallas_call x1, Pallas kernels, on_device(): pl.pallas_call(functools.partial(attention_kernel, n_ep, heads * n_tp), o...  4.37 us
    pallas_call x1, Pallas kernels, on_device(): pl.pallas_call(functools.partial(expert_kernel, n_ep, n_tp), out_shape=sh...  1.34 us
  transfers between devices with their start and end apart: 14, of which 12 were waited for; matrix products, arithmetic and copies ran while one was open for 0% of the time, Pallas kernels for 0%

profile of v1, /device:TPU:0, one launch (start us, length us, event | category | flops | bytes accessed | tf_op | source)
XLA Modules:
  0.0 56.1 jit_solution(11810576528562492761)
XLA Ops:
  0.7 1.0 %slices.1 = (bf16[16,1024]{1,0:T(8,128)(2,1)S(1)}, bf16[16,1024]{1,0:T(8,128)(2,1)S(1)}, bf16[16,1024]{1,0:T(8,128)(2,1)S(1)}, bf16[16,1024]{1,0:T(8,128)(2,1)S(1)}) custom-call(bf16[16,4096]{1,0:T(8,128)(2,1)} %tokens.1, f32[1,4096]{1,0:T(1,128)} %bitcast.25), custom_call_target="tpu_custom_call" | custom-call | flops 20000000000 | bytes 1048576 | tf_op jit(solution)/shard_map/slices/pallas_call | solution.py:288
  1.7 2.5 %collective-permute-start = (bf16[16,1024]{1,0:T(8,128)(2,1)S(1)}, bf16[16,1024]{1,0:T(8,128)(2,1)S(1)}, u32[]{:S(2)}, u32[]{:S(2)}) collective-permute-start(bf16[16,1024]{1,0:T(8,128)(2,1)S(1)} %get-tuple-element.25), channel_id=1, source_target_pairs={{0,9},{1,8},{2,11},{3,10},{4,13},{5,12},{6,15},{7,14},{8,1},{9,0},... | collective-permute-start | bytes 98312 | tf_op jit(solution)/shard_map/ppermute | solution.py:283
  4.2 1.8 %collective-permute-start.1 = (bf16[16,1024]{1,0:T(8,128)(2,1)S(1)}, bf16[16,1024]{1,0:T(8,128)(2,1)S(1)}, u32[]{:S(2)}, u32[]{:S(2)}) collective-permute-start(bf16[16,1024]{1,0:T(8,128)(2,1)S(1)} %get-tuple-element.26), channel_id=1, source_target_pairs={{0,17},{1,16},{2,19},{3,18},{4,21},{5,20},{6,23},{7,22},{8,25},{9,... | collective-permute-start | bytes 98312 | tf_op jit(solution)/shard_map/ppermute | solution.py:283
  6.0 0.0 collective-permute-start.2
  6.1 0.2 tables.1
  6.2 1.4 %collective-permute-done.1.refs_2_ = bf16[16,1024]{1,0:T(8,128)(2,1)S(1)} collective-permute-done((bf16[16,1024]{1,0:T(8,128)(2,1)S(1)}, bf16[16,1024]{1,0:T(8,128)(2,1)S(1)}, u32[]{:S(2)}, u32[]{:S(2)}) %collective-permute-start.1) | collective-permute-done | bytes 32800 | tf_op jit(solution)/shard_map/ppermute | solution.py:283
  7.6 3.0 %collective-permute-done.2.refs_3_ = bf16[16,1024]{1,0:T(8,128)(2,1)S(1)} collective-permute-done((bf16[16,1024]{1,0:T(8,128)(2,1)S(1)}, bf16[16,1024]{1,0:T(8,128)(2,1)S(1)}, u32[]{:S(2)}, u32[]{:S(2)}) %collective-permute-start.2) | collective-permute-done | bytes 32800 | tf_op jit(solution)/shard_map/ppermute | solution.py:283
  10.6 0.0 slice-start.1
  10.7 0.4 project.1
  11.1 0.5 collective-permute-start.3
  11.6 0.1 collective-permute-start.4
  11.7 3.0 %collective-permute-start.5 = (f32[16,768]{1,0:T(8,128)S(1)}, f32[16,768]{1,0:T(8,128)S(1)}, u32[]{:S(2)}, u32[]{:S(2)}) collective-permute-start(f32[16,768]{1,0:T(8,128)S(1)} %get-tuple-element.32), channel_id=1, source_target_pairs={{0,24},{8,16},{16,8},{24,0},{1,25},{9,17},{17,9},{25,1},{2,26},{10... | collective-permute-start | bytes 147464 | tf_op jit(solution)/shard_map/ppermute | solution.py:274
  14.6 0.6 %collective-permute-done.3.refs_1_ = f32[16,768]{1,0:T(8,128)S(1)} collective-permute-done((f32[16,768]{1,0:T(8,128)S(1)}, f32[16,768]{1,0:T(8,128)S(1)}, u32[]{:S(2)}, u32[]{:S(2)}) %collective-permute-start.3) | collective-permute-done | bytes 49184 | tf_op jit(solution)/shard_map/ppermute | solution.py:274
  15.3 0.9 %collective-permute-done.4.refs_2_ = f32[16,768]{1,0:T(8,128)S(1)} collective-permute-done((f32[16,768]{1,0:T(8,128)S(1)}, f32[16,768]{1,0:T(8,128)S(1)}, u32[]{:S(2)}, u32[]{:S(2)}) %collective-permute-start.4) | collective-permute-done | bytes 49184 | tf_op jit(solution)/shard_map/ppermute | solution.py:274
  16.1 0.6 collective-permute-done.5.refs_3_
  16.8 4.4 %attention.1 = (bf16[16,2048]{1,0:T(8,128)(2,1)S(1)}, bf16[16,2048]{1,0:T(8,128)(2,1)S(1)}, bf16[16,256]{1,0:T(8,128)(2,1)}, bf16[16,256]{1,0:T(8,128)(2,1)}) custom-call(s32[1,16]{1,0:T(1,128)S(1)} %bitcast.22, f32[1,2]{1,0:T(1,128)S(1)} %bitcast.23, f32[16,768]{1,0:T(8,128)S(1)} %get-tuple-element.29.refs_0_, ...), custom_call_target="tpu_custom_call" | custom-call | flops 10000000000 | bytes 1048576 | tf_op jit(solution)/shard_map/attention/pallas_call | solution.py:322
  21.2 1.3 %collective-permute-done.6.got = bf16[16,2048]{1,0:T(8,128)(2,1)S(1)} collective-permute-done((bf16[16,2048]{1,0:T(8,128)(2,1)S(1)}, bf16[16,2048]{1,0:T(8,128)(2,1)S(1)}, u32[]{:S(2)}, u32[]{:S(2)}) %collective-permute-start.6) | collective-permute-done | bytes 65568 | tf_op jit(solution)/shard_map/ppermute | solution.py:274
  22.4 4.0 %collective-permute-start.9 = (bf16[16,2048]{1,0:T(8,128)(2,1)S(1)}, bf16[16,2048]{1,0:T(8,128)(2,1)S(1)}, u32[]{:S(2)}, u32[]{:S(2)}) collective-permute-start(bf16[16,2048]{1,0:T(8,128)(2,1)S(1)} %pair.1.refs_0_), channel_id=1, source_target_pairs={{0,6},{1,7},{2,4},{3,5},{4,2},{5,3},{6,0},{7,1},{8,14},{9,15},{10,... | collective-permute-start | bytes 196616 | tf_op jit(solution)/shard_map/ppermute | solution.py:274
  26.5 0.6 %collective-permute-start.7 = (bf16[16,2048]{1,0:T(8,128)(2,1)S(1)}, bf16[16,2048]{1,0:T(8,128)(2,1)S(1)}, u32[]{:S(2)}, u32[]{:S(2)}) collective-permute-start(bf16[16,2048]{1,0:T(8,128)(2,1)S(1)} %pair.1.refs_0_), channel_id=1, source_target_pairs={{0,2},{1,3},{2,0},{3,1},{4,6},{5,7},{6,4},{7,5},{8,10},{9,11},{10,... | collective-permute-start | bytes 196616 | tf_op jit(solution)/shard_map/ppermute | solution.py:274
  27.1 2.0 %collective-permute-done.9.refs_3_ = bf16[16,2048]{1,0:T(8,128)(2,1)S(1)} collective-permute-done((bf16[16,2048]{1,0:T(8,128)(2,1)S(1)}, bf16[16,2048]{1,0:T(8,128)(2,1)S(1)}, u32[]{:S(2)}, u32[]{:S(2)}) %collective-permute-start.9) | collective-permute-done | bytes 65568 | tf_op jit(solution)/shard_map/ppermute | solution.py:274
  29.1 3.3 %collective-permute-done.8.refs_2_ = bf16[16,2048]{1,0:T(8,128)(2,1)S(1)} collective-permute-done((bf16[16,2048]{1,0:T(8,128)(2,1)S(1)}, bf16[16,2048]{1,0:T(8,128)(2,1)S(1)}, u32[]{:S(2)}, u32[]{:S(2)}) %collective-permute-start.8) | collective-permute-done | bytes 65568 | tf_op jit(solution)/shard_map/ppermute | solution.py:274
  32.4 0.2 dispatch.1
  32.6 0.9 %collective-permute-start.10 = (bf16[8,2048]{1,0:T(8,128)(2,1)S(1)}, bf16[8,2048]{1,0:T(8,128)(2,1)S(1)}, u32[]{:S(2)}, u32[]{:S(2)}) collective-permute-start(bf16[8,2048]{1,0:T(8,128)(2,1)S(1)} %get-tuple-element.36), channel_id=1, source_target_pairs={{0,9},{1,8},{2,11},{3,10},{4,13},{5,12},{6,15},{7,14},{8,1},{9,0},... | collective-permute-start | bytes 98312 | tf_op jit(solution)/shard_map/ppermute | solution.py:283
  33.5 2.0 %collective-permute-start.11 = (bf16[8,2048]{1,0:T(8,128)(2,1)S(1)}, bf16[8,2048]{1,0:T(8,128)(2,1)S(1)}, u32[]{:S(2)}, u32[]{:S(2)}) collective-permute-start(bf16[8,2048]{1,0:T(8,128)(2,1)S(1)} %get-tuple-element.37), channel_id=1, source_target_pairs={{0,17},{1,16},{2,19},{3,18},{4,21},{5,20},{6,23},{7,22},{8,25},{9,... | collective-permute-start | bytes 98312 | tf_op jit(solution)/shard_map/ppermute | solution.py:283
  35.5 0.8 %collective-permute-done.10.refs_1_ = bf16[8,2048]{1,0:T(8,128)(2,1)S(1)} collective-permute-done((bf16[8,2048]{1,0:T(8,128)(2,1)S(1)}, bf16[8,2048]{1,0:T(8,128)(2,1)S(1)}, u32[]{:S(2)}, u32[]{:S(2)}) %collective-permute-start.10) | collective-permute-done | bytes 32800 | tf_op jit(solution)/shard_map/ppermute | solution.py:283
  36.2 0.8 %collective-permute-done.11.refs_2_ = bf16[8,2048]{1,0:T(8,128)(2,1)S(1)} collective-permute-done((bf16[8,2048]{1,0:T(8,128)(2,1)S(1)}, bf16[8,2048]{1,0:T(8,128)(2,1)S(1)}, u32[]{:S(2)}, u32[]{:S(2)}) %collective-permute-start.11) | collective-permute-done | bytes 32800 | tf_op jit(solution)/shard_map/ppermute | solution.py:283
  37.1 2.9 %collective-permute-done.12.refs_3_ = bf16[8,2048]{1,0:T(8,128)(2,1)S(1)} collective-permute-done((bf16[8,2048]{1,0:T(8,128)(2,1)S(1)}, bf16[8,2048]{1,0:T(8,128)(2,1)S(1)}, u32[]{:S(2)}, u32[]{:S(2)}) %collective-permute-start.12) | collective-permute-done | bytes 32800 | tf_op jit(solution)/shard_map/ppermute | solution.py:283
  40.0 0.1 collective-permute-start.13
  40.1 1.3 %collective-permute-done.13.theirs = bf16[32,2048]{1,0:T(8,128)(2,1)S(1)} collective-permute-done((bf16[32,2048]{1,0:T(8,128)(2,1)S(1)}, bf16[32,2048]{1,0:T(8,128)(2,1)S(1)}, u32[]{:S(2)}, u32[]{:S(2)}) %collective-permute-start.13) | collective-permute-done | bytes 131104 | tf_op jit(solution)/shard_map/ppermute | solution.py:274
  41.4 1.3 %experts.1 = bf16[4,64,512]{2,1,0:T(8,128)(2,1)S(1)} custom-call(bf16[32,2048]{1,0:T(8,128)(2,1)S(1)} %stack.1.mine, bf16[32,2048]{1,0:T(8,128)(2,1)S(1)} %collective-permute-done.13.theirs, f32[1,4096]{1,0:T(1,128)S(1)} %bitcast.17, bf16[1,4096,256]{2,1,0:T(8,128)(2,1)S(1)} %copy-done.1, bf16[1,4096,256]{2,1,0:T(8,128)(2,1)S(1)} %copy-done.2, ...), custom_call_target="tpu_custom_call" | custom-call | flops 5000000000 | bytes 1048576 | tf_op jit(solution)/shard_map/experts/pallas_call | solution.py:368
  42.7 12.5 %all_to_all.11 = bf16[32,8,512]{2,1,0:T(8,128)(2,1)S(1)} all-to-all(bf16[32,8,512]{2,1,0:T(8,128)(2,1)S(1)} %bitcast.12), channel_id=1, replica_groups=mesh['ep'=4,'tp'=8] {'ep','tp'}, dimensions={0} | all-to-all | bytes 524288 | tf_op jit(solution)/shard_map/all_to_all | solution.py:378
  55.3 0.8 %combine.1 = bf16[16,512]{1,0:T(8,128)(2,1)} custom-call(bf16[256,512]{1,0:T(8,128)(2,1)S(1)} %bitcast.11, f32[16,512]{1,0:T(8,128)S(1)} %get-tuple-element.39.resid, bf16[32,32]{1,0:T(8,128)(2,1)S(1)} %get-tuple-element.40.picks, f32[32,128]{1,0:T(8,128)S(1)} %get-tuple-element.28.refs_7_.shares), custom_call_target="tpu_custom_call" | custom-call | flops 1000000000 | bytes 1048576 | tf_op jit(solution)/shard_map/combine/pallas_call | solution.py:379
  (48 shorter events, 0.2 us)
Async XLA Ops:
  0.6 5.4 %copy-start.9 = (s32[16,2]{0,1:T(2,128)S(1)}, s32[16,2]{0,1:T(2,128)}, u32[]{:S(2)}) copy-start(s32[16,2]{0,1:T(2,128)} %param.32) | copy-start | bytes 388
  0.6 5.4 %copy-start.10 = (f32[16,2]{0,1:T(2,128)S(1)}, f32[16,2]{0,1:T(2,128)}, u32[]{:S(2)}) copy-start(f32[16,2]{0,1:T(2,128)} %param.34) | copy-start | bytes 388
  1.7 8.9 %copy-start.4 = (bf16[1024,256]{1,0:T(8,128)(2,1)S(1)}, bf16[1024,256]{1,0:T(8,128)(2,1)}, u32[]{:S(2)}) copy-start(bf16[1024,256]{1,0:T(8,128)(2,1)} %refs_4_.1) | copy-start | bytes 1572868
  1.7 8.9 %copy-start.5 = (bf16[1024,256]{1,0:T(8,128)(2,1)S(1)}, bf16[1024,256]{1,0:T(8,128)(2,1)}, u32[]{:S(2)}) copy-start(bf16[1024,256]{1,0:T(8,128)(2,1)} %refs_5_.2) | copy-start | bytes 1572868
  1.7 8.9 %copy-start.6 = (bf16[1024,256]{1,0:T(8,128)(2,1)S(1)}, bf16[1024,256]{1,0:T(8,128)(2,1)}, u32[]{:S(2)}) copy-start(bf16[1024,256]{1,0:T(8,128)(2,1)} %refs_6_.2) | copy-start | bytes 1572868
  1.7 4.5 %collective-permute-start = (bf16[16,1024]{1,0:T(8,128)(2,1)S(1)}, bf16[16,1024]{1,0:T(8,128)(2,1)S(1)}, u32[]{:S(2)}, u32[]{:S(2)}) collective-permute-start(bf16[16,1024]{1,0:T(8,128)(2,1)S(1)} %get-tuple-element.25), channel_id=1, source_target_pairs={{0,9},{1,8},{2,11},{3,10},{4,13},{5,12},{6,15},{7,14},{8,1},{9,0},... | collective-permute-start | bytes 98312 | tf_op jit(solution)/shard_map/ppermute | solution.py:283
  4.2 3.4 %collective-permute-start.1 = (bf16[16,1024]{1,0:T(8,128)(2,1)S(1)}, bf16[16,1024]{1,0:T(8,128)(2,1)S(1)}, u32[]{:S(2)}, u32[]{:S(2)}) collective-permute-start(bf16[16,1024]{1,0:T(8,128)(2,1)S(1)} %get-tuple-element.26), channel_id=1, source_target_pairs={{0,17},{1,16},{2,19},{3,18},{4,21},{5,20},{6,23},{7,22},{8,25},{9,... | collective-permute-start | bytes 98312 | tf_op jit(solution)/shard_map/ppermute | solution.py:283
  6.0 4.6 %collective-permute-start.2 = (bf16[16,1024]{1,0:T(8,128)(2,1)S(1)}, bf16[16,1024]{1,0:T(8,128)(2,1)S(1)}, u32[]{:S(2)}, u32[]{:S(2)}) collective-permute-start(bf16[16,1024]{1,0:T(8,128)(2,1)S(1)} %get-tuple-element.27), channel_id=1, source_target_pairs={{0,25},{1,24},{2,27},{3,26},{4,29},{5,28},{6,31},{7,30},{8,17},{9,... | collective-permute-start | bytes 98312 | tf_op jit(solution)/shard_map/ppermute | solution.py:283
  6.1 10.6 %slice-start = ((s8[8388608]{0:T(1024)(128)(4,1)}), s8[4194304]{0:T(1024)(128)(4,1)S(1)}, s32[]{:S(2)}) async-start(s8[8388608]{0:T(1024)(128)(4,1)} %bitcast.13), calls=%async_computation.1 | async-start | bytes 8388608
  6.1 10.6 %slice-start.2 = ((s8[8388608]{0:T(1024)(128)(4,1)}), s8[4194304]{0:T(1024)(128)(4,1)S(1)}, s32[]{:S(2)}) async-start(s8[8388608]{0:T(1024)(128)(4,1)} %bitcast.15), calls=%async_computation.3 | async-start | bytes 8388608
  10.6 6.1 %slice-start.1 = ((s8[8388608]{0:T(1024)(128)(4,1)}), s8[4194304]{0:T(1024)(128)(4,1)S(1)}, s32[]{:S(2)}) async-start(s8[8388608]{0:T(1024)(128)(4,1)} %bitcast.13), calls=%async_computation.2 | async-start | bytes 8388608
  10.6 6.1 %slice-start.3 = ((s8[8388608]{0:T(1024)(128)(4,1)}), s8[4194304]{0:T(1024)(128)(4,1)S(1)}, s32[]{:S(2)}) async-start(s8[8388608]{0:T(1024)(128)(4,1)} %bitcast.15), calls=%async_computation.4 | async-start | bytes 8388608
  10.6 6.1 %copy-start = (bf16[256,4096]{1,0:T(8,128)(2,1)S(1)}, bf16[256,4096]{1,0:T(8,128)(2,1)}, u32[]{:S(2)}) copy-start(bf16[256,4096]{1,0:T(8,128)(2,1)} %refs_7_.1) | copy-start | bytes 6291460
  10.6 6.1 %copy-start.13 = (s32[16]{0:T(128)S(1)}, s32[16]{0:T(128)}, u32[]{:S(2)}) copy-start(s32[16]{0:T(128)} %param.29) | copy-start | bytes 196
  10.7 6.1 %copy-start.14 = (f32[2]{0:T(128)S(1)}, f32[2]{0:T(128)}, u32[]{:S(2)}) copy-start(f32[2]{0:T(128)} %param.24) | copy-start | bytes 28
  10.7 6.1 %copy-start.15 = (f32[128]{0:T(128)S(1)}, f32[128]{0:T(128)}, u32[]{:S(2)}) copy-start(f32[128]{0:T(128)} %param.25) | copy-start | bytes 1540
  11.1 4.2 %collective-permute-start.3 = (f32[16,768]{1,0:T(8,128)S(1)}, f32[16,768]{1,0:T(8,128)S(1)}, u32[]{:S(2)}, u32[]{:S(2)}) collective-permute-start(f32[16,768]{1,0:T(8,128)S(1)} %get-tuple-element.30), channel_id=1, source_target_pairs={{0,8},{8,0},{16,24},{24,16},{1,9},{9,1},{17,25},{25,17},{2,10},{10... | collective-permute-start | bytes 147464 | tf_op jit(solution)/shard_map/ppermute | solution.py:274
  11.6 4.6 %collective-permute-start.4 = (f32[16,768]{1,0:T(8,128)S(1)}, f32[16,768]{1,0:T(8,128)S(1)}, u32[]{:S(2)}, u32[]{:S(2)}) collective-permute-start(f32[16,768]{1,0:T(8,128)S(1)} %get-tuple-element.31), channel_id=1, source_target_pairs={{0,16},{8,24},{16,0},{24,8},{1,17},{9,25},{17,1},{25,9},{2,18},{10... | collective-permute-start | bytes 147464 | tf_op jit(solution)/shard_map/ppermute | solution.py:274
  11.7 5.0 %collective-permute-start.5 = (f32[16,768]{1,0:T(8,128)S(1)}, f32[16,768]{1,0:T(8,128)S(1)}, u32[]{:S(2)}, u32[]{:S(2)}) collective-permute-start(f32[16,768]{1,0:T(8,128)S(1)} %get-tuple-element.32), channel_id=1, source_target_pairs={{0,24},{8,16},{16,8},{24,0},{1,25},{9,17},{17,9},{25,1},{2,26},{10... | collective-permute-start | bytes 147464 | tf_op jit(solution)/shard_map/ppermute | solution.py:274
  16.8 15.6 %copy-start.7 = (bf16[16,4096]{1,0:T(8,128)(2,1)S(1)}, bf16[16,4096]{1,0:T(8,128)(2,1)}, u32[]{:S(2)}) copy-start(bf16[16,4096]{1,0:T(8,128)(2,1)} %tokens.1) | copy-start | bytes 393220
  21.2 1.3 %collective-permute-start.6 = (bf16[16,2048]{1,0:T(8,128)(2,1)S(1)}, bf16[16,2048]{1,0:T(8,128)(2,1)S(1)}, u32[]{:S(2)}, u32[]{:S(2)}) collective-permute-start(bf16[16,2048]{1,0:T(8,128)(2,1)S(1)} %get-tuple-element.34), channel_id=1, source_target_pairs={{0,1},{1,0},{2,3},{3,2},{4,5},{5,4},{6,7},{7,6},{8,9},{9,8},{10,11... | collective-permute-start | bytes 196616 | tf_op jit(solution)/shard_map/ppermute | solution.py:274
  22.4 6.7 %collective-permute-start.9 = (bf16[16,2048]{1,0:T(8,128)(2,1)S(1)}, bf16[16,2048]{1,0:T(8,128)(2,1)S(1)}, u32[]{:S(2)}, u32[]{:S(2)}) collective-permute-start(bf16[16,2048]{1,0:T(8,128)(2,1)S(1)} %pair.1.refs_0_), channel_id=1, source_target_pairs={{0,6},{1,7},{2,4},{3,5},{4,2},{5,3},{6,0},{7,1},{8,14},{9,15},{10,... | collective-permute-start | bytes 196616 | tf_op jit(solution)/shard_map/ppermute | solution.py:274
  26.5 5.9 %collective-permute-start.8 = (bf16[16,2048]{1,0:T(8,128)(2,1)S(1)}, bf16[16,2048]{1,0:T(8,128)(2,1)S(1)}, u32[]{:S(2)}, u32[]{:S(2)}) collective-permute-start(bf16[16,2048]{1,0:T(8,128)(2,1)S(1)} %pair.1.refs_0_), channel_id=1, source_target_pairs={{0,4},{1,5},{2,6},{3,7},{4,0},{5,1},{6,2},{7,3},{8,12},{9,13},{10,... | collective-permute-start | bytes 196616 | tf_op jit(solution)/shard_map/ppermute | solution.py:274
  26.5 5.9 %collective-permute-start.7 = (bf16[16,2048]{1,0:T(8,128)(2,1)S(1)}, bf16[16,2048]{1,0:T(8,128)(2,1)S(1)}, u32[]{:S(2)}, u32[]{:S(2)}) collective-permute-start(bf16[16,2048]{1,0:T(8,128)(2,1)S(1)} %pair.1.refs_0_), channel_id=1, source_target_pairs={{0,2},{1,3},{2,0},{3,1},{4,6},{5,7},{6,4},{7,5},{8,10},{9,11},{10,... | collective-permute-start | bytes 196616 | tf_op jit(solution)/shard_map/ppermute | solution.py:274
  32.4 9.0 %copy-start.1 = (bf16[1,4096,256]{2,1,0:T(8,128)(2,1)S(1)}, bf16[1,4096,256]{2,1,0:T(8,128)(2,1)}, u32[]{:S(2)}) copy-start(bf16[1,4096,256]{2,1,0:T(8,128)(2,1)} %w_gate.1) | copy-start | bytes 6291460
  32.4 9.0 %copy-start.2 = (bf16[1,4096,256]{2,1,0:T(8,128)(2,1)S(1)}, bf16[1,4096,256]{2,1,0:T(8,128)(2,1)}, u32[]{:S(2)}) copy-start(bf16[1,4096,256]{2,1,0:T(8,128)(2,1)} %w_up.1) | copy-start | bytes 6291460
  32.4 9.0 %copy-start.3 = (bf16[1,256,4096]{2,1,0:T(8,128)(2,1)S(1)}, bf16[1,256,4096]{2,1,0:T(8,128)(2,1)}, u32[]{:S(2)}) copy-start(bf16[1,256,4096]{2,1,0:T(8,128)(2,1)} %w_down.1) | copy-start | bytes 6291460
  32.4 9.0 %copy-start.8 = (f32[4096]{0:T(1024)S(1)}, f32[4096]{0:T(1024)}, u32[]{:S(2)}) copy-start(f32[4096]{0:T(1024)} %param.30) | copy-start | bytes 49156
  32.6 3.7 %collective-permute-start.10 = (bf16[8,2048]{1,0:T(8,128)(2,1)S(1)}, bf16[8,2048]{1,0:T(8,128)(2,1)S(1)}, u32[]{:S(2)}, u32[]{:S(2)}) collective-permute-start(bf16[8,2048]{1,0:T(8,128)(2,1)S(1)} %get-tuple-element.36), channel_id=1, source_target_pairs={{0,9},{1,8},{2,11},{3,10},{4,13},{5,12},{6,15},{7,14},{8,1},{9,0},... | collective-permute-start | bytes 98312 | tf_op jit(solution)/shard_map/ppermute | solution.py:283
  33.5 3.6 %collective-permute-start.11 = (bf16[8,2048]{1,0:T(8,128)(2,1)S(1)}, bf16[8,2048]{1,0:T(8,128)(2,1)S(1)}, u32[]{:S(2)}, u32[]{:S(2)}) collective-permute-start(bf16[8,2048]{1,0:T(8,128)(2,1)S(1)} %get-tuple-element.37), channel_id=1, source_target_pairs={{0,17},{1,16},{2,19},{3,18},{4,21},{5,20},{6,23},{7,22},{8,25},{9,... | collective-permute-start | bytes 98312 | tf_op jit(solution)/shard_map/ppermute | solution.py:283
  35.5 4.5 %collective-permute-start.12 = (bf16[8,2048]{1,0:T(8,128)(2,1)S(1)}, bf16[8,2048]{1,0:T(8,128)(2,1)S(1)}, u32[]{:S(2)}, u32[]{:S(2)}) collective-permute-start(bf16[8,2048]{1,0:T(8,128)(2,1)S(1)} %get-tuple-element.38), channel_id=1, source_target_pairs={{0,25},{1,24},{2,27},{3,26},{4,29},{5,28},{6,31},{7,30},{8,17},{9,... | collective-permute-start | bytes 98312 | tf_op jit(solution)/shard_map/ppermute | solution.py:283
  40.0 1.4 %collective-permute-start.13 = (bf16[32,2048]{1,0:T(8,128)(2,1)S(1)}, bf16[32,2048]{1,0:T(8,128)(2,1)S(1)}, u32[]{:S(2)}, u32[]{:S(2)}) collective-permute-start(bf16[32,2048]{1,0:T(8,128)(2,1)S(1)} %stack.1.mine), channel_id=1, source_target_pairs={{0,1},{1,0},{2,3},{3,2},{4,5},{5,4},{6,7},{7,6},{8,9},{9,8},{10,11... | collective-permute-start | bytes 393224 | tf_op jit(solution)/shard_map/ppermute | solution.py:274
  (2 other events, 10.8 us)
